TPU v7x, 32 devices: a whole 2x2x4 slice. The times are simulated.
32 devices in a mesh: row: 8 (over z, core), col: 4 (over y, x).
Axes of the slice: x: 2, y: 2, z: 4, core: 2. Of those that a mesh axis runs over, the one named last changes fastest.
Arguments:
- tokens: bfloat16 [4096, 4096], P('row', 'col'), may hold values from -6 to 6
- norm_gain: float32 [4096], replicated, may hold values from 0.1 to 1.9
- out_weight: bfloat16 [4096, 4096], P(None, 'col'), may hold values from -0.09375 to 0.09375
Outputs:
- mixed: bfloat16 [4096, 4096], P('row', 'col')
All inputs are finite; a program needn't handle non-finite values.
Results may differ from a plain program's by a relative error of at most 0.015.
Values may be sent and summed in bfloat16 or wider, within the bound.
No kernel may reach another device: no remote copies, remote signals or barrier semaphores. Data moves between devices by JAX's collectives and lax.ppermute only.
A program may use at most 64 MiB of HBM per device.

v0:
```python
import math

import jax
import jax.numpy as jnp
from jax import lax
from jax.sharding import PartitionSpec as P

GROUPS = 4


EPSILON = 1e-06
PRECISE = lax.Precision.HIGHEST


def phases(left_idx, right_idx, period):
    product = left_idx[:, None] * right_idx[None, :] % period
    angles = product.astype(jnp.float32) * (2.0 * math.pi / period)
    return (jnp.cos(angles), jnp.sin(angles))


def split_table(table):
    table_high = table.astype(jnp.bfloat16)
    remainder = table - table_high.astype(jnp.float32)
    table_middle = remainder.astype(jnp.bfloat16)
    table_low = (remainder - table_middle.astype(jnp.float32)).astype(jnp.bfloat16)
    return (table_high, table_middle, table_low)


def on_device(tokens, norm_gain, out_weight):
    row_count = lax.axis_size("row")
    col_count = lax.axis_size("col")
    block_len, local_width = tokens.shape
    full_width = local_width * col_count
    group_len = full_width // GROUPS
    share_len = block_len // col_count
    seq_len = block_len * row_count
    slab_len = full_width // row_count
    col_index = lax.axis_index("col")
    chan_idx = jnp.arange(group_len, dtype=jnp.int32)
    cosines, sines = phases(chan_idx, chan_idx, group_len)
    chan_table = jnp.concatenate([cosines, sines], axis=1) / math.sqrt(group_len)
    table_parts = split_table(chan_table)
    arranged = tokens.reshape(col_count, share_len, local_width)
    portion = lax.all_to_all(arranged, "col", split_axis=0, concat_axis=2, tiled=True)
    item_count = portion.shape[1]
    values = portion.astype(jnp.float32)
    inv_rms = lax.rsqrt(jnp.mean(values * values, axis=-1, keepdims=True) + EPSILON)
    normed = lax.optimization_barrier((values * inv_rms * norm_gain).astype(jnp.bfloat16))
    grouped = normed.reshape(item_count, GROUPS, group_len)
    result = jnp.einsum("pgm,mj->pgj", grouped, table_parts[0], preferred_element_type=jnp.float32)
    result = result + jnp.einsum(
        "pgm,mj->pgj", grouped, table_parts[1], preferred_element_type=jnp.float32
    )
    result = result + jnp.einsum(
        "pgm,mj->pgj", grouped, table_parts[2], preferred_element_type=jnp.float32
    )
    high_idx = jnp.arange(row_count, dtype=jnp.int32)
    high_cos, high_sin = phases(high_idx, high_idx, row_count)
    high_table = jnp.concatenate(
        [jnp.concatenate([high_cos, -high_sin], 1), jnp.concatenate([-high_sin, -high_cos], 1)], 0
    )
    parts = (
        lax.all_to_all(
            result[..., :group_len].reshape(1, item_count, full_width),
            "row",
            split_axis=2,
            concat_axis=0,
            tiled=True,
        ),
        lax.all_to_all(
            result[..., group_len:].reshape(1, item_count, full_width),
            "row",
            split_axis=2,
            concat_axis=0,
            tiled=True,
        ),
    )
    item_count = parts[0].shape[1]
    stacked = jnp.concatenate(parts, 0).reshape(2 * row_count, item_count * slab_len)
    result = jnp.dot(high_table, stacked, precision=PRECISE)
    real_part = result[:row_count].reshape(row_count, item_count, slab_len)
    imag_part = result[row_count:].reshape(row_count, item_count, slab_len)
    local_pos = col_index * share_len + jnp.arange(share_len, dtype=jnp.int32)
    twist_cos, twist_sin = phases(high_idx, local_pos, seq_len)
    twist_cos = twist_cos[:, :, None]
    twist_sin = twist_sin[:, :, None]
    turned_real = real_part * twist_cos + imag_part * twist_sin
    turned_imag = imag_part * twist_cos - real_part * twist_sin
    low_idx = jnp.arange(block_len, dtype=jnp.int32)
    low_cos, low_sin = phases(low_idx, low_idx, block_len)
    low_cos = low_cos / math.sqrt(seq_len)
    low_sin = low_sin / math.sqrt(seq_len)
    low_table = jnp.concatenate([low_cos, low_sin], 1)
    stacked = jnp.concatenate(
        (
            lax.all_to_all(turned_real, "col", split_axis=0, concat_axis=1, tiled=True),
            lax.all_to_all(turned_imag, "col", split_axis=0, concat_axis=1, tiled=True),
        ),
        1,
    )
    finished = (jnp.einsum("ks,asc->akc", low_table, stacked, precision=PRECISE),)[0]
    spectrum = finished.astype(jnp.bfloat16)
    returned = lax.all_to_all(spectrum, "row", split_axis=1, concat_axis=2, tiled=True)
    mapped = jnp.einsum(
        "akd,de->kae",
        lax.all_gather(returned, "col", axis=0, tiled=True),
        out_weight,
        preferred_element_type=jnp.float32,
    )
    return mapped.astype(jnp.bfloat16).reshape(block_len, local_width)


def solution(mesh):
    placed = (P("row", "col"), P(), P(None, "col"))
    return jax.shard_map(
        on_device, mesh=mesh, in_specs=placed, out_specs=P("row", "col"), check_vma=False
    )
```

profile of v0, /device:TPU:9, one launch (start us, length us, event | category | flops | bytes accessed | tf_op | source)
XLA Modules:
  0.0 339.9 jit_solution(3100324161421210881)
XLA Ops:
  6.5 3.5 %all-to-all-start = ((bf16[4,128,1024]{2,1,0:T(8,128)(2,1)}), bf16[4,128,1024]{2,1,0:T(8,128)(2,1)S(1)}, u32[]{:S(2)}, u32[]{:S(2)}) async-start(bf16[4,128,1024]{2,1,0:T(8,128)(2,1)} %bitcast.99), calls=%async_computation | async-start | bytes 2097152 | tf_op jit(solution)/shard_map/all_to_all | solution.py:44
  10.1 17.6 %fusion.34 = (f32[1024,1024]{1,0:T(8,128)}, f32[1024,1024]{1,0:T(8,128)}) fusion(), kind=kLoop, calls=%fused_computation.43 | loop fusion | flops 14680064 | bytes 8388608 | tf_op jit(solution)/shard_map/sin | solution.py:18
  29.3 1.9 copy.49
  33.4 4.7 %fusion.4 = f32[128,4,2048]{2,0,1:T(8,128)S(1)} fusion(bf16[128,4,1024]{0,2,1:T(8,128)(2,1)S(1)} %bitcast.81, f32[1024,1024]{1,0:T(8,128)S(1)} %copy-done, f32[1024,1024]{1,0:T(8,128)} %get-tuple-element.14), kind=kOutput, calls=%fused_computation.10 | convolution fusion | flops 2153775104 | bytes 13631488 | tf_op jit(solution)/shard_map/pgm,mj->pgj/dot_general | solution.py:50
  38.1 2.4 fusion.10
  40.5 2.5 add_add_fusion
  43.0 1.8 fusion.88
  44.7 1.8 copy.53
  46.6 5.8 %all-to-all-start.1 = ((f32[1,128,4096]{1,0,2:T(1,128)}), f32[1,128,4096]{1,0,2:T(1,128)S(1)}, u32[]{:S(2)}, u32[]{:S(2)}) async-start(f32[1,128,4096]{1,0,2:T(1,128)} %bitcast.90), calls=%async_computation.1 | async-start | bytes 4194304 | tf_op jit(solution)/shard_map/all_to_all | solution.py:63
  52.4 2.9 copy.56
  55.3 42.6 %all-to-all-done.1 = f32[1,128,4096]{1,0,2:T(1,128)S(1)} async-done(((f32[1,128,4096]{1,0,2:T(1,128)}), f32[1,128,4096]{1,0,2:T(1,128)S(1)}, u32[]{:S(2)}, u32[]{:S(2)}) %all-to-all-start.1) | async-done | bytes 2097184 | tf_op jit(solution)/shard_map/all_to_all | solution.py:63
  97.9 7.7 %all-to-all-start.2 = ((f32[1,128,4096]{1,0,2:T(1,128)}), f32[1,128,4096]{1,0,2:T(1,128)}, u32[]{:S(2)}, u32[]{:S(2)}) async-start(f32[1,128,4096]{1,0,2:T(1,128)} %bitcast.87), calls=%async_computation.2 | async-start | bytes 4194304 | tf_op jit(solution)/shard_map/all_to_all | solution.py:70
  105.8 1.9 copy.55
  107.7 2.8 copy.73
  110.5 40.7 %all-to-all-done.2 = f32[1,128,4096]{1,0,2:T(1,128)} async-done(((f32[1,128,4096]{1,0,2:T(1,128)}), f32[1,128,4096]{1,0,2:T(1,128)}, u32[]{:S(2)}, u32[]{:S(2)}) %all-to-all-start.2) | async-done | bytes 2097184 | tf_op jit(solution)/shard_map/all_to_all | solution.py:70
  151.2 2.9 copy.58
  154.1 2.8 copy.74
  156.9 3.8 %fusion.12 = f32[16,65536]{1,0:T(8,128)S(1)} fusion(f32[8,65536]{1,0:T(8,128)S(1)} %bitcast.85, f32[8,65536]{1,0:T(8,128)S(1)} %bitcast.84, f32[8,8]{1,0:T(8,128)S(1)} %fusion.78, f32[8,8]{1,0:T(8,128)S(1)} %get-tuple-element.15, f32[8,8]{1,0:T(8,128)S(1)} %get-tuple-element.16), kind=kOutput, calls=%fused_computation.16 | convolution fusion | flops 202375936 | bytes 8389376 | tf_op jit(solution)/shard_map/dot_general | solution.py:80
  161.0 3.7 %multiply_add_fusion = (f32[8,128,512]{2,1,0:T(8,128)S(1)}, f32[8,128,512]{2,1,0:T(8,128)}) fusion(f32[8,128,512]{2,0,1:T(8,128)S(1)} %bitcast.92, f32[8,128,512]{2,0,1:T(8,128)S(1)} %bitcast.91, f32[8,128]{1,0:T(8,128)S(1)} %get-tuple-element.12, f32[8,128]{1,0:T(8,128)S(1)} %get-tuple-element.11), kind=kLoop, calls=%fused_computation.42 | loop fusion | flops 3145728 | bytes 8396800 | tf_op jit(solution)/shard_map/add | solution.py:87
  164.7 28.0 %all_to_all.93 = f32[8,128,512]{2,1,0:T(8,128)} all-to-all(f32[8,128,512]{2,1,0:T(8,128)S(1)} %get-tuple-element.5), channel_id=1, replica_groups=mesh['row'=8,'col'=4] {'col'}, dimensions={0} | all-to-all | bytes 4194304 | tf_op jit(solution)/shard_map/all_to_all | solution.py:96
  192.7 3.6 %all-to-all-start.4 = ((f32[8,128,512]{2,1,0:T(8,128)}), f32[8,128,512]{2,1,0:T(8,128)S(1)}, u32[]{:S(2)}, u32[]{:S(2)}) async-start(f32[8,128,512]{2,1,0:T(8,128)} %get-tuple-element.6), calls=%async_computation.4 | async-start | bytes 4194304 | tf_op jit(solution)/shard_map/all_to_all | solution.py:97
  196.6 5.3 %sine_multiply_fusion = (f32[512,512]{1,0:T(8,128)S(1)}, f32[512,512]{1,0:T(8,128)}) fusion(), kind=kLoop, calls=%fused_computation.56 | loop fusion | flops 4194304 | bytes 2097152 | tf_op jit(solution)/shard_map/div | solution.py:92
  201.9 2.9 copy.61
  204.8 3.1 all_to_all.78
  207.9 12.8 %all-to-all-done.4 = f32[8,128,512]{2,1,0:T(8,128)S(1)} async-done(((f32[8,128,512]{2,1,0:T(8,128)}), f32[8,128,512]{2,1,0:T(8,128)S(1)}, u32[]{:S(2)}, u32[]{:S(2)}) %all-to-all-start.4) | async-done | bytes 2097184 | tf_op jit(solution)/shard_map/all_to_all | solution.py:97
  220.6 1.8 copy.64
  222.5 3.2 all_to_all.82
  225.7 9.6 %fusion.44 = bf16[2,512,512]{1,2,0:T(8,128)(2,1)} fusion(f32[512,512]{1,0:T(8,128)S(1)} %get-tuple-element.17, f32[512,512]{1,0:T(8,128)} %get-tuple-element.18, f32[2,512,512]{1,2,0:T(8,128)} %all_to_all.82, f32[2,512,512]{1,2,0:T(8,128)S(1)} %copy-done.2), kind=kOutput, calls=%fused_computation.50 | convolution fusion | flops 6444548096 | bytes 7340032 | tf_op jit(solution)/shard_map/ks,asc->akc/dot_general | solution.py:101
  235.3 2.5 copy.65
  237.8 30.5 %all_to_all.94 = bf16[2,512,512]{2,0,1:T(2,128)(2,1)S(1)} all-to-all(bf16[2,512,512]{2,0,1:T(2,128)(2,1)S(1)} %copy.65), channel_id=1, replica_groups=mesh['row'=8,'col'=4] {'row'}, dimensions={1} | all-to-all | bytes 2097152 | tf_op jit(solution)/shard_map/all_to_all | solution.py:103
  269.6 52.7 %all-gather.2.cloned.1.call-done = bf16[8,64,4096]{2,1,0:T(8,128)(2,1)} async-done(((bf16[2,64,4096]{2,1,0:T(8,128)(2,1)}), bf16[8,64,4096]{2,1,0:T(8,128)(2,1)}) %all-gather.2.cloned.1.call-update) | async-done | bytes 4194320 | tf_op jit(solution)/shard_map/all_gather | solution.py:106
  322.3 9.1 %fusion.47 = bf16[64,8,1024]{2,0,1:T(8,128)(2,1)S(1)} fusion(bf16[8,64,4096]{2,1,0:T(8,128)(2,1)} %all-gather.2.cloned.1.call-done, bf16[4096,1024]{1,0:T(8,128)(2,1)} %param.5), kind=kOutput, calls=%fused_computation.51 | convolution fusion | flops 4295491584 | bytes 13631488 | tf_op jit(solution)/shard_map/akd,de->kae/dot_general | solution.py:104
  (23 shorter events, 7.3 us)
Async XLA Ops:
  6.5 21.1 %all-to-all-start = ((bf16[4,128,1024]{2,1,0:T(8,128)(2,1)}), bf16[4,128,1024]{2,1,0:T(8,128)(2,1)S(1)}, u32[]{:S(2)}, u32[]{:S(2)}) async-start(bf16[4,128,1024]{2,1,0:T(8,128)(2,1)} %bitcast.99), calls=%async_computation | async-start | bytes 2097152 | tf_op jit(solution)/shard_map/all_to_all | solution.py:44
  27.6 3.9 %copy-start.3 = (f32[4096]{0:T(1024)S(1)}, f32[4096]{0:T(1024)}, u32[]{:S(2)}) copy-start(f32[4096]{0:T(1024)} %param.4) | copy-start | bytes 49156
  31.2 2.2 copy-start
  33.4 4.7 %copy-start.1 = (f32[1024,1024]{1,0:T(8,128)S(1)}, f32[1024,1024]{1,0:T(8,128)}, u32[]{:S(2)}) copy-start(f32[1024,1024]{1,0:T(8,128)} %get-tuple-element.14) | copy-start | bytes 12582916
  46.6 51.3 %all-to-all-start.1 = ((f32[1,128,4096]{1,0,2:T(1,128)}), f32[1,128,4096]{1,0,2:T(1,128)S(1)}, u32[]{:S(2)}, u32[]{:S(2)}) async-start(f32[1,128,4096]{1,0,2:T(1,128)} %bitcast.90), calls=%async_computation.1 | async-start | bytes 4194304 | tf_op jit(solution)/shard_map/all_to_all | solution.py:63
  97.9 53.3 %all-to-all-start.2 = ((f32[1,128,4096]{1,0,2:T(1,128)}), f32[1,128,4096]{1,0,2:T(1,128)}, u32[]{:S(2)}, u32[]{:S(2)}) async-start(f32[1,128,4096]{1,0,2:T(1,128)} %bitcast.87), calls=%async_computation.2 | async-start | bytes 4194304 | tf_op jit(solution)/shard_map/all_to_all | solution.py:70
  192.7 28.0 %all-to-all-start.4 = ((f32[8,128,512]{2,1,0:T(8,128)}), f32[8,128,512]{2,1,0:T(8,128)S(1)}, u32[]{:S(2)}, u32[]{:S(2)}) async-start(f32[8,128,512]{2,1,0:T(8,128)} %get-tuple-element.6), calls=%async_computation.4 | async-start | bytes 4194304 | tf_op jit(solution)/shard_map/all_to_all | solution.py:97
  196.3 126.1 %all-gather.2.cloned.1.call-start = ((), (), s32[]{:S(2)}) async-start(), calls=%async_computation.6 | async-start | bytes 5242880 | tf_op jit(solution)/shard_map/all_gather | solution.py:106
  222.5 3.2 copy-start.2
Sparse Core Ops, SparseCore 0:
  269.8 52.5 all-gather.1
where the time goes:
time: 342 us; the launch traced here: 340 us
  waiting for transfers between devices  149 us (44%)
  blocking collectives  58.5 us (17%)
  local copies, waits for them, and re-layouts  36.4 us (11%)
  matrix products  32.1 us (9%)
  other arithmetic  29.6 us (9%)
  starting transfers between devices  20.9 us (6%)
  between operations  13.5 us (4%)
    all_gather x1, waiting for transfers between devices, on_device(): lax.all_gather(returned, 'col', axis=0, tiled=True)  52.7 us
    all_to_all x1, waiting for transfers between devices, on_device(): lax.all_to_all(result[..., :group_len].reshape(1, item_count, full_width)...  42.6 us
    all_to_all x1, waiting for transfers between devices, on_device(): lax.all_to_all(result[..., group_len:].reshape(1, item_count, full_width)...  40.7 us
    all_to_all x1, blocking collectives, on_device(): lax.all_to_all(spectrum, 'row', split_axis=1, concat_axis=2, tiled=True)  30.5 us
    all_to_all x1, blocking collectives, on_device(): lax.all_to_all(turned_real, 'col', split_axis=0, concat_axis=1, tiled=True)  28 us
    sin x1, other arithmetic, phases(): return (jnp.cos(angles), jnp.sin(angles))  17.6 us
    all_to_all x1, waiting for transfers between devices, on_device(): lax.all_to_all(turned_imag, 'col', split_axis=0, concat_axis=1, tiled=True)  12.8 us
    dot_general x1, matrix products, on_device(): jnp.einsum('ks,asc->akc', low_table, stacked, precision=PRECISE)  9.62 us
  transfers between devices with their start and end apart: 5, of which 4 were waited for; matrix products, arithmetic and copies ran while one was open for 10% of the time, Pallas kernels for 0%

commit v1 on v0

--- a/solution.py
+++ b/solution.py
@@ -110,8 +110,148 @@
     return mapped.astype(jnp.bfloat16).reshape(block_len, local_width)
 
 
+def cosines_of(product, period, phase=0.0):
+    return jnp.cos((product % period).astype(jnp.float32) * (2.0 * math.pi / period) - phase)
+
+
+def channel_table(row_count, width):
+    slab = width // row_count
+    half = slab // 2
+    coarse_len = 1 << (width.bit_length() // 2)
+    lane = jnp.arange(width, dtype=jnp.int32)
+    in_slab = lane % slab
+    freq = (lane // slab) * half + in_slab % half
+    is_sine = in_slab >= half
+    packed = is_sine & (freq == 0)
+    freq = jnp.where(packed, width // 2, freq)[None, :]
+    quarter = jnp.where(is_sine & ~packed, 0.5 * math.pi, 0.0)[None, :]
+    coarse = jnp.arange(0, width, coarse_len, dtype=jnp.int32)[:, None]
+    fine = jnp.arange(coarse_len, dtype=jnp.int32)[:, None]
+    scale = 1.0 / math.sqrt(width)
+    coarse_cos = cosines_of(coarse * freq, width)
+    coarse_sin = cosines_of(coarse * freq, width, 0.5 * math.pi)
+    fine_cos = cosines_of(fine * freq, width, quarter) * scale
+    fine_sin = cosines_of(fine * freq, width, quarter + 0.5 * math.pi) * scale
+    table = (
+        coarse_cos[:, None, :] * fine_cos[None] - coarse_sin[:, None, :] * fine_sin[None]
+    )
+    return table.astype(jnp.bfloat16).reshape(width, width)
+
+
+def folding_matrix(row_index, row_count, width):
+    slab = width // row_count
+    half = slab // 2
+    out_idx = jnp.arange(width, dtype=jnp.int32)[:, None]
+    source = (row_index - out_idx // slab) % row_count
+    in_slab = out_idx % slab
+    freq = source * half + in_slab % half
+    is_sine = in_slab >= half
+    packed = is_sine & (freq == 0)
+    freq = jnp.where(packed, width // 2, freq)
+    sign = jnp.where(is_sine & ~packed, -1.0, 1.0)
+    chan = jnp.arange(width, dtype=jnp.int32)[None, :]
+    straight = jnp.where(chan == freq, sign, 0.0)
+    mirrored = jnp.where((chan == (width - freq) % width) & (chan != freq), 1.0, 0.0)
+    return (straight + mirrored).astype(jnp.bfloat16)
+
+
+def on_device_whole_groups(tokens, norm_gain, out_weight):
+    row_count = lax.axis_size("row")
+    col_count = lax.axis_size("col")
+    block_len, width = tokens.shape
+    full_width = width * col_count
+    slab = width // row_count
+    half = slab // 2
+    seq_len = block_len * row_count
+    low_len = block_len // row_count
+    row_index = lax.axis_index("row")
+    col_index = lax.axis_index("col")
+
+    def across_col(value, flip):
+        return lax.ppermute(value, "col", [(k, k ^ flip) for k in range(col_count)])
+
+    def along_row(value, shift):
+        return lax.ppermute(
+            value, "row", [(k, (k + shift) % row_count) for k in range(row_count)]
+        )
+
+    values = tokens.astype(jnp.float32)
+    squares = jnp.sum(values * values, axis=-1)
+    total = squares
+    for flip in range(1, col_count):
+        total = total + across_col(squares, flip)
+    inv_rms = lax.rsqrt(total / full_width + EPSILON)
+    gain = lax.dynamic_slice(norm_gain, (col_index * width,), (width,))
+    gained = (values * gain).astype(jnp.bfloat16)
+    chan = jnp.dot(gained, channel_table(row_count, width), preferred_element_type=jnp.float32)
+    chan = (chan * inv_rms[:, None]).astype(jnp.bfloat16)
+    chan = chan.reshape(block_len, row_count, slab).transpose(1, 0, 2)
+
+    def to_row(blocks, shift):
+        return lax.dynamic_index_in_dim(blocks, (row_index + shift) % row_count, 0, keepdims=False)
+
+    got = [to_row(chan, 0)]
+    for shift in range(1, row_count):
+        got.append(along_row(to_row(chan, shift), shift))
+
+    wide = [value.astype(jnp.float32) for value in got]
+    local_pos = row_index * block_len + jnp.arange(block_len, dtype=jnp.int32)
+    lane = jnp.arange(slab, dtype=jnp.int32)
+    takes_sine = (lane >= half) & ~((lane == half) & (row_index == 0))
+    reals, imags = [], []
+    for high in range(row_count):
+        part_cos = 0.0
+        part_sin = 0.0
+        for shift in range(row_count):
+            angle = 2.0 * math.pi * (shift * high % row_count) / row_count
+            part_cos = part_cos + round(math.cos(angle), 15) * wide[shift]
+            part_sin = part_sin + round(math.sin(angle), 15) * wide[shift]
+        twist = (high * local_pos % seq_len).astype(jnp.float32) * (2.0 * math.pi / seq_len)
+        twist_cos = jnp.cos(twist)[:, None]
+        twist_sin = jnp.sin(twist)[:, None]
+        real = part_cos * twist_cos + part_sin * twist_sin
+        imag = part_sin * twist_cos - part_cos * twist_sin
+        reals.append(jnp.where(takes_sine, -imag, real).astype(jnp.bfloat16))
+        imags.append(jnp.where(takes_sine, real, imag).astype(jnp.bfloat16))
+    stacked = jnp.concatenate(
+        [jnp.concatenate(reals, axis=1), jnp.concatenate(imags, axis=1)], axis=0
+    )
+    low_idx = jnp.arange(block_len, dtype=jnp.int32)
+    low_cos, low_sin = phases(low_idx, low_idx, block_len)
+    low_table = jnp.concatenate([low_cos, low_sin], 1) / math.sqrt(seq_len)
+    spectrum = jnp.dot(
+        low_table.astype(jnp.bfloat16), stacked, preferred_element_type=jnp.float32
+    ).astype(jnp.bfloat16)
+    spectrum = spectrum.reshape(row_count, low_len, row_count * slab)
+    back = [to_row(spectrum, 0)]
+    for shift in range(1, row_count):
+        back.append(along_row(to_row(spectrum, shift), shift))
+    own = jnp.stack(back)
+
+    fold = folding_matrix(row_index, row_count, width)
+    weights = []
+    for flip in range(col_count):
+        rows = lax.dynamic_slice(out_weight, ((col_index ^ flip) * width, 0), (width, width))
+        weights.append(
+            jnp.dot(fold, rows, preferred_element_type=jnp.float32).astype(jnp.bfloat16)
+        )
+
+    next_x = across_col(own, 1)
+    next_y = across_col(own, 2)
+    cut = row_count // 2
+    far = jnp.concatenate([across_col(next_y[:cut], 1), across_col(next_x[cut:], 2)], 0)
+    mixed = 0.0
+    for part, weight in zip((own, next_x, next_y, far), weights):
+        part = part.reshape(row_count, low_len, row_count, slab)
+        part = part.transpose(1, 2, 0, 3).reshape(block_len, width)
+        mixed = mixed + jnp.dot(part, weight, preferred_element_type=jnp.float32)
+    return mixed.astype(jnp.bfloat16)
+
+
 def solution(mesh):
     placed = (P("row", "col"), P(), P(None, "col"))
+    whole_groups = mesh.shape["col"] == GROUPS == 4
+    body = on_device_whole_groups if whole_groups else on_device
     return jax.shard_map(
-        on_device, mesh=mesh, in_specs=placed, out_specs=P("row", "col"), check_vma=False
-    )
+        body, mesh=mesh, in_specs=placed, out_specs=P("row", "col"), check_vma=False
+    )

time: 342 us -> 134 us (0.39)
  waiting for transfers between devices: 149 us -> 46 us
  blocking collectives: 58.5 us -> 0 us
  local copies, waits for them, and re-layouts: 36.4 us -> 15 us
  other arithmetic: 29.6 us -> 16.2 us
  between operations: 13.5 us -> 0.56 us
    all_to_all x4 -> x0, waiting for transfers between devices: 96.1 us -> none  [the longest x1 42.6 us: on_device(): lax.all_to_all(result[..., :group_len].reshape(1, item_count, full_width)...]
    all_to_all x2 -> x0, blocking collectives: 58.5 us -> none  [the longest x1 30.5 us: on_device(): lax.all_to_all(spectrum, 'row', split_axis=1, concat_axis=2, tiled=True)]
    all_gather x1 -> x0, waiting for transfers between devices: 52.7 us -> none  [on_device(): lax.all_gather(returned, 'col', axis=0, tiled=True)]
    ppermute x0 -> x21, waiting for transfers between devices: none -> 46 us  [the longest x14 32.2 us: along_row(): lax.ppermute(value, 'row', [(k, (k + shift) % row_count) for k in range(r...]
    ppermute x0 -> x21, starting transfers between devices: none -> 23.9 us  [the longest x14 15.9 us: along_row(): lax.ppermute(value, 'row', [(k, (k + shift) % row_count) for k in range(r...]
    all_to_all x4 -> x0, starting transfers between devices: 20.6 us -> none  [the longest x1 7.73 us: on_device(): lax.all_to_all(result[..., group_len:].reshape(1, item_count, full_width)...]
    all_to_all x8 -> x0, local copies, waits for them, and re-layouts: 17.1 us -> none  [the longest x2 5.99 us: on_device(): lax.all_to_all(turned_real, 'col', split_axis=0, concat_axis=1, tiled=True)]
    sin x1, other arithmetic: 17.6 us -> 4.94 us  [phases(): return (jnp.cos(angles), jnp.sin(angles))]
  transfers between devices with their start and end apart: 5 -> 21, of which waited for: 4 -> 10; matrix products, arithmetic and copies ran while one was open for 10% -> 29% of each run, Pallas kernels for 0% -> 0%
where the time goes in v1:
time: 134 us
  waiting for transfers between devices  46 us (34%)
  matrix products  32 us (24%)
  starting transfers between devices  23.9 us (18%)
  other arithmetic  16.2 us (12%)
  local copies, waits for them, and re-layouts  15 us (11%)
    ppermute x14, waiting for transfers between devices, along_row(): lax.ppermute(value, 'row', [(k, (k + shift) % row_count) for k in range(r...  32.2 us
    dot_general x4, matrix products, on_device_whole_groups(): mixed = mixed + jnp.dot(part, weight, preferred_element_type=jnp.float32)  29.5 us
    ppermute x14, starting transfers between devices, along_row(): lax.ppermute(value, 'row', [(k, (k + shift) % row_count) for k in range(r...  15.9 us
    ppermute x7, waiting for transfers between devices, across_col(): return lax.ppermute(value, 'col', [(k, k ^ flip) for k in range(col_count)])  13.8 us
    ppermute x7, starting transfers between devices, across_col(): return lax.ppermute(value, 'col', [(k, k ^ flip) for k in range(col_count)])  8.03 us
    unnamed x41, local copies, waits for them, and re-layouts  6.31 us
    transpose x7, local copies, waits for them, and re-layouts, on_device_whole_groups(): part = part.transpose(1, 2, 0, 3).reshape(block_len, width)  5.09 us
    sin x1, other arithmetic, phases(): return (jnp.cos(angles), jnp.sin(angles))  4.94 us
  transfers between devices with their start and end apart: 21, of which 10 were waited for; matrix products, arithmetic and copies ran while one was open for 29% of the time, Pallas kernels for 0%

profile of v1, /device:TPU:9, one launch (start us, length us, event | category | flops | bytes accessed | tf_op | source)
XLA Modules:
  0.0 133.7 jit_solution(18333346696836789777)
XLA Ops:
  0.0 1.6 %fusion.2 = f32[512]{0:T(512)S(1)} fusion(bf16[512,1024]{1,0:T(8,128)(2,1)} %param.3), kind=kLoop, calls=%fused_computation.9 | loop fusion | flops 1572352 | bytes 1050624 | tf_op jit(solution)/shard_map/reduce_sum | solution.py:179
  1.6 1.3 collective-permute-start
  2.9 1.2 collective-permute-start.1
  4.6 4.9 %fusion.74 = (f32[512,512]{1,0:T(8,128)}, f32[512,512]{1,0:T(8,128)}) fusion(), kind=kLoop, calls=%fused_computation.125 | loop fusion | flops 3670016 | bytes 2097152 | tf_op jit(solution)/shard_map/sin | solution.py:18
  9.5 1.8 %fusion.170 = (f32[32,1024]{1,0:T(8,128)S(1)}, f32[32,1024]{1,0:T(8,128)S(1)}, f32[32,1024]{1,0:T(8,128)S(1)}, f32[32,1024]{1,0:T(8,128)S(1)}) fusion(s32[1024]{0:T(1024)S(1)} %fusion.196, s32[32]{0:T(128)S(1)} %iota_multiply_fusion, f32[1024]{0:T(1024)S(1)} %broadcast_add_fusion, f32[1024]{0:T(1024)S(1)} %get-tuple-element.55), kind=kLoop, calls=%fused_computation.296 | loop fusion | flops 1081344 | bytes 536704 | tf_op jit(solution)/shard_map/cos | solution.py:114
  13.0 1.3 fusion.48
  14.5 2.2 %constant_dynamic-slice_fusion.7 = (bf16[512,1,128]{2,1,0:T(2,128)(2,1)S(1)}, bf16[512,1,128]{2,1,0:T(2,128)(2,1)S(1)}, bf16[512,1,128]{2,1,0:T(2,128)(2,1)S(1)}...) fusion(bf16[512,8,128]{2,1,0:T(8,128)(2,1)S(1)} %bitcast.154, ...), kind=kLoop, calls=%fused_computation.325 | loop fusion | bytes 2097184 | tf_op jit(solution)/shard_map/dynamic-slice
  16.7 2.7 %collective-permute-start.3 = (bf16[512,128]{1,0:T(8,128)(2,1)S(1)}, bf16[512,128]{1,0:T(8,128)(2,1)S(1)}, u32[]{:S(2)}, u32[]{:S(2)}) collective-permute-start(bf16[512,128]{1,0:T(8,128)(2,1)S(1)} %bitcast.182), channel_id=1, source_target_pairs={{0,4},{4,8},{8,12},{12,16},{16,20},{20,24},{24,28},{28,0},{1,5},{5... | collective-permute-start | bytes 393224 | tf_op jit(solution)/shard_map/ppermute | solution.py:174
  19.5 1.3 %collective-permute-start.4 = (bf16[512,128]{1,0:T(8,128)(2,1)S(1)}, bf16[512,128]{1,0:T(8,128)(2,1)S(1)}, u32[]{:S(2)}, u32[]{:S(2)}) collective-permute-start(bf16[512,128]{1,0:T(8,128)(2,1)S(1)} %bitcast.180), channel_id=1, source_target_pairs={{0,8},{4,12},{8,16},{12,20},{16,24},{20,28},{24,0},{28,4},{1,9},{5... | collective-permute-start | bytes 393224 | tf_op jit(solution)/shard_map/ppermute | solution.py:174
  21.1 1.4 %collective-permute-start.6 = (bf16[512,128]{1,0:T(8,128)(2,1)S(1)}, bf16[512,128]{1,0:T(8,128)(2,1)S(1)}, u32[]{:S(2)}, u32[]{:S(2)}) collective-permute-start(bf16[512,128]{1,0:T(8,128)(2,1)S(1)} %bitcast.181), channel_id=1, source_target_pairs={{0,16},{4,20},{8,24},{12,28},{16,0},{20,4},{24,8},{28,12},{1,17},{... | collective-permute-start | bytes 393224 | tf_op jit(solution)/shard_map/ppermute | solution.py:174
  22.5 1.7 %collective-permute-start.7 = (bf16[512,128]{1,0:T(8,128)(2,1)S(1)}, bf16[512,128]{1,0:T(8,128)(2,1)S(1)}, u32[]{:S(2)}, u32[]{:S(2)}) collective-permute-start(bf16[512,128]{1,0:T(8,128)(2,1)S(1)} %bitcast.183), channel_id=1, source_target_pairs={{0,20},{4,24},{8,28},{12,0},{16,4},{20,8},{24,12},{28,16},{1,21},{... | collective-permute-start | bytes 393224 | tf_op jit(solution)/shard_map/ppermute | solution.py:174
  25.9 13.1 %collective-permute-done.5 = bf16[512,128]{1,0:T(8,128)(2,1)S(1)} collective-permute-done((bf16[512,128]{1,0:T(8,128)(2,1)S(1)}, bf16[512,128]{1,0:T(8,128)(2,1)S(1)}, u32[]{:S(2)}, u32[]{:S(2)}) %collective-permute-start.5) | collective-permute-done | bytes 131104 | tf_op jit(solution)/shard_map/ppermute | solution.py:174
  39.0 2.8 %collective-permute-done.6 = bf16[512,128]{1,0:T(8,128)(2,1)S(1)} collective-permute-done((bf16[512,128]{1,0:T(8,128)(2,1)S(1)}, bf16[512,128]{1,0:T(8,128)(2,1)S(1)}, u32[]{:S(2)}, u32[]{:S(2)}) %collective-permute-start.6) | collective-permute-done | bytes 131104 | tf_op jit(solution)/shard_map/ppermute | solution.py:174
  41.8 1.5 %collective-permute-done.8 = bf16[512,128]{1,0:T(8,128)(2,1)S(1)} collective-permute-done((bf16[512,128]{1,0:T(8,128)(2,1)S(1)}, bf16[512,128]{1,0:T(8,128)(2,1)S(1)}, u32[]{:S(2)}, u32[]{:S(2)}) %collective-permute-start.8) | collective-permute-done | bytes 131104 | tf_op jit(solution)/shard_map/ppermute | solution.py:174
  48.6 1.3 fusion.24
  51.4 1.7 %collective-permute-start.12 = (bf16[64,1024]{1,0:T(8,128)(2,1)S(1)}, bf16[64,1024]{1,0:T(8,128)(2,1)S(1)}, u32[]{:S(2)}, u32[]{:S(2)}) collective-permute-start(bf16[64,1024]{1,0:T(8,128)(2,1)S(1)} %get-tuple-element.35), channel_id=1, source_target_pairs={{0,12},{4,16},{8,20},{12,24},{16,28},{20,0},{24,4},{28,8},{1,13},{... | collective-permute-start | bytes 393224 | tf_op jit(solution)/shard_map/ppermute | solution.py:174
  53.7 2.0 %collective-permute-start.14 = (bf16[64,1024]{1,0:T(8,128)(2,1)S(1)}, bf16[64,1024]{1,0:T(8,128)(2,1)S(1)}, u32[]{:S(2)}, u32[]{:S(2)}) collective-permute-start(bf16[64,1024]{1,0:T(8,128)(2,1)S(1)} %get-tuple-element.33), channel_id=1, source_target_pairs={{0,20},{4,24},{8,28},{12,0},{16,4},{20,8},{24,12},{28,16},{1,21},{... | collective-permute-start | bytes 393224 | tf_op jit(solution)/shard_map/ppermute | solution.py:174
  55.8 1.4 %collective-permute-start.15 = (bf16[64,1024]{1,0:T(8,128)(2,1)S(1)}, bf16[64,1024]{1,0:T(8,128)(2,1)S(1)}, u32[]{:S(2)}, u32[]{:S(2)}) collective-permute-start(bf16[64,1024]{1,0:T(8,128)(2,1)S(1)} %get-tuple-element.32), channel_id=1, source_target_pairs={{0,24},{4,28},{8,0},{12,4},{16,8},{20,12},{24,16},{28,20},{1,25},{... | collective-permute-start | bytes 393224 | tf_op jit(solution)/shard_map/ppermute | solution.py:174
  59.3 10.8 %collective-permute-done.12 = bf16[64,1024]{1,0:T(8,128)(2,1)S(1)} collective-permute-done((bf16[64,1024]{1,0:T(8,128)(2,1)S(1)}, bf16[64,1024]{1,0:T(8,128)(2,1)S(1)}, u32[]{:S(2)}, u32[]{:S(2)}) %collective-permute-start.12) | collective-permute-done | bytes 131104 | tf_op jit(solution)/shard_map/ppermute | solution.py:174
  70.8 2.1 %collective-permute-done.13 = bf16[64,1024]{1,0:T(8,128)(2,1)S(1)} collective-permute-done((bf16[64,1024]{1,0:T(8,128)(2,1)S(1)}, bf16[64,1024]{1,0:T(8,128)(2,1)S(1)}, u32[]{:S(2)}, u32[]{:S(2)}) %collective-permute-start.13) | collective-permute-done | bytes 131104 | tf_op jit(solution)/shard_map/ppermute | solution.py:174
  74.3 1.7 %collective-permute-done.15 = bf16[64,1024]{1,0:T(8,128)(2,1)S(1)} collective-permute-done((bf16[64,1024]{1,0:T(8,128)(2,1)S(1)}, bf16[64,1024]{1,0:T(8,128)(2,1)S(1)}, u32[]{:S(2)}, u32[]{:S(2)}) %collective-permute-start.15) | collective-permute-done | bytes 131104 | tf_op jit(solution)/shard_map/ppermute | solution.py:174
  77.3 1.3 collective-permute-start.18
  80.1 1.2 copy.80
  81.4 7.0 %fusion.20 = f32[512,1024]{1,0:T(8,128)} fusion(bf16[4096,1024]{1,0:T(8,128)(2,1)} %param.5, s32[]{:T(128)S(6)} %select_n.438, s32[1024]{0:T(1024)S(1)} %get-tuple-element.52, f32[1024]{0:T(1024)S(1)} %get-tuple-element.54, s32[1024]{0:T(1024)S(1)} %get-tuple-element.53, bf16[64,8,8,128]{3,2,1,0:T(8,128)(2,1)S(1)} %copy.80), kind=kOutput, calls=%fused_computation.29 | convolution fusion | flops 3230662656 | bytes 5255172 | tf_op jit(solution)/shard_map/dot_general | solution.py:247
  88.4 13.6 %collective-permute-done.18 = bf16[8,64,1024]{2,1,0:T(8,128)(2,1)S(1)} collective-permute-done((bf16[8,64,1024]{2,1,0:T(8,128)(2,1)}, bf16[8,64,1024]{2,1,0:T(8,128)(2,1)S(1)}, u32[]{:S(2)}, u32[]{:S(2)}) %collective-permute-start.18) | collective-permute-done | bytes 1048608 | tf_op jit(solution)/shard_map/ppermute | solution.py:171
  102.0 1.7 %collective-permute-start.19 = (bf16[4,64,1024]{2,1,0:T(8,128)(2,1)S(1)}, bf16[4,64,1024]{2,1,0:T(8,128)(2,1)}, u32[]{:S(2)}, u32[]{:S(2)}) collective-permute-start(bf16[4,64,1024]{2,1,0:T(8,128)(2,1)S(1)} %slice.8), channel_id=1, source_target_pairs={{0,1},{1,0},{2,3},{3,2},{4,5},{5,4},{6,7},{7,6},{8,9},{9,8},{10,11... | collective-permute-start | bytes 1572872 | tf_op jit(solution)/shard_map/ppermute | solution.py:171
  105.4 1.2 copy.79
  108.2 7.1 %fusion.16 = f32[512,1024]{1,0:T(8,128)} fusion(bf16[4096,1024]{1,0:T(8,128)(2,1)} %param.5, s32[]{:T(128)S(6)} %select_n.491, s32[1024]{0:T(1024)S(1)} %get-tuple-element.52, f32[1024]{0:T(1024)S(1)} %get-tuple-element.54, s32[1024]{0:T(1024)S(1)} %get-tuple-element.53, bf16[64,8,8,128]{3,2,1,0:T(8,128)(2,1)S(1)} %copy.79), kind=kOutput, calls=%fused_computation.25 | convolution fusion | flops 3230662656 | bytes 5255172 | tf_op jit(solution)/shard_map/dot_general | solution.py:247
  115.4 7.2 %fusion.12 = f32[512,1024]{1,0:T(8,128)} fusion(bf16[4096,1024]{1,0:T(8,128)(2,1)} %param.5, s32[]{:T(128)S(6)} %select_n.492, s32[1024]{0:T(1024)S(1)} %get-tuple-element.52, f32[1024]{0:T(1024)S(1)} %get-tuple-element.54, s32[1024]{0:T(1024)S(1)} %get-tuple-element.53, bf16[64,8,8,128]{3,2,1,0:T(8,128)(2,1)S(1)} %copy.78), kind=kOutput, calls=%fused_computation.21 | convolution fusion | flops 3230662656 | bytes 5255172 | tf_op jit(solution)/shard_map/dot_general | solution.py:247
  122.6 1.4 %pad_maximum_fusion = bf16[8,64,1024]{2,1,0:T(8,128)(2,1)S(1)} fusion(bf16[4,64,1024]{2,1,0:T(8,128)(2,1)} %collective-permute-done.20, bf16[4,64,1024]{2,1,0:T(8,128)(2,1)} %collective-permute-done.19), kind=kLoop, calls=%fused_computation.54 | loop fusion | flops 524288 | bytes 2097152 | tf_op jit(solution)/shard_map/concatenate | solution.py:242
  124.4 1.2 copy.77
  125.7 8.1 %add_convert_fusion.1 = bf16[512,1024]{1,0:T(8,128)(2,1)} fusion(f32[512,1024]{1,0:T(8,128)} %fusion.12, f32[512,1024]{1,0:T(8,128)S(1)} %copy-done.3, f32[512,1024]{1,0:T(8,128)} %fusion.16, bf16[4096,1024]{1,0:T(8,128)(2,1)} %param.5, s32[]{:T(128)S(6)} %select_n.493, s32[1024]{0:T(1024)S(1)} %get-tuple-element.52, f32[1024]{0:T(1024)S(1)} %get-tuple-element.54, ...), kind=kOutput, calls=%fused_computation.16 | convolution fusion | flops 3232759808 | bytes 10498052 | tf_op jit(solution)/shard_map/dot_general | solution.py:247
  (103 shorter events, 22.1 us)
Async XLA Ops:
  0.0 13.0 %copy-start = (bf16[512,1024]{1,0:T(8,128)(2,1)S(1)}, bf16[512,1024]{1,0:T(8,128)(2,1)}, u32[]{:S(2)}) copy-start(bf16[512,1024]{1,0:T(8,128)(2,1)} %param.3) | copy-start | bytes 3145732
  1.6 11.4 %collective-permute-start = (f32[512]{0:T(512)S(1)}, f32[512]{0:T(512)S(1)}, u32[]{:S(2)}, u32[]{:S(2)}) collective-permute-start(f32[512]{0:T(512)S(1)} %fusion.2), channel_id=1, source_target_pairs={{0,1},{1,0},{2,3},{3,2},{4,5},{5,4},{6,7},{7,6},{8,9},{9,8},{10,11... | collective-permute-start | bytes 6152 | tf_op jit(solution)/shard_map/ppermute | solution.py:171
  2.9 10.1 %collective-permute-start.1 = (f32[512]{0:T(512)S(1)}, f32[512]{0:T(512)S(1)}, u32[]{:S(2)}, u32[]{:S(2)}) collective-permute-start(f32[512]{0:T(512)S(1)} %fusion.2), channel_id=1, source_target_pairs={{0,2},{1,3},{2,0},{3,1},{4,6},{5,7},{6,4},{7,5},{8,10},{9,11},{10,... | collective-permute-start | bytes 6152 | tf_op jit(solution)/shard_map/ppermute | solution.py:171
  4.1 8.8 %collective-permute-start.2 = (f32[512]{0:T(512)S(1)}, f32[512]{0:T(512)S(1)}, u32[]{:S(2)}, u32[]{:S(2)}) collective-permute-start(f32[512]{0:T(512)S(1)} %fusion.2), channel_id=1, source_target_pairs={{0,3},{1,2},{2,1},{3,0},{4,7},{5,6},{6,5},{7,4},{8,11},{9,10},{10,... | collective-permute-start | bytes 6152 | tf_op jit(solution)/shard_map/ppermute | solution.py:171
  16.7 7.5 %collective-permute-start.3 = (bf16[512,128]{1,0:T(8,128)(2,1)S(1)}, bf16[512,128]{1,0:T(8,128)(2,1)S(1)}, u32[]{:S(2)}, u32[]{:S(2)}) collective-permute-start(bf16[512,128]{1,0:T(8,128)(2,1)S(1)} %bitcast.182), channel_id=1, source_target_pairs={{0,4},{4,8},{8,12},{12,16},{16,20},{20,24},{24,28},{28,0},{1,5},{5... | collective-permute-start | bytes 393224 | tf_op jit(solution)/shard_map/ppermute | solution.py:174
  19.5 6.0 %collective-permute-start.4 = (bf16[512,128]{1,0:T(8,128)(2,1)S(1)}, bf16[512,128]{1,0:T(8,128)(2,1)S(1)}, u32[]{:S(2)}, u32[]{:S(2)}) collective-permute-start(bf16[512,128]{1,0:T(8,128)(2,1)S(1)} %bitcast.180), channel_id=1, source_target_pairs={{0,8},{4,12},{8,16},{12,20},{16,24},{20,28},{24,0},{28,4},{1,9},{5... | collective-permute-start | bytes 393224 | tf_op jit(solution)/shard_map/ppermute | solution.py:174
  21.0 18.0 %collective-permute-start.5 = (bf16[512,128]{1,0:T(8,128)(2,1)S(1)}, bf16[512,128]{1,0:T(8,128)(2,1)S(1)}, u32[]{:S(2)}, u32[]{:S(2)}) collective-permute-start(bf16[512,128]{1,0:T(8,128)(2,1)S(1)} %bitcast.179), channel_id=1, source_target_pairs={{0,12},{4,16},{8,20},{12,24},{16,28},{20,0},{24,4},{28,8},{1,13},{... | collective-permute-start | bytes 393224 | tf_op jit(solution)/shard_map/ppermute | solution.py:174
  21.1 20.7 %collective-permute-start.6 = (bf16[512,128]{1,0:T(8,128)(2,1)S(1)}, bf16[512,128]{1,0:T(8,128)(2,1)S(1)}, u32[]{:S(2)}, u32[]{:S(2)}) collective-permute-start(bf16[512,128]{1,0:T(8,128)(2,1)S(1)} %bitcast.181), channel_id=1, source_target_pairs={{0,16},{4,20},{8,24},{12,28},{16,0},{20,4},{24,8},{28,12},{1,17},{... | collective-permute-start | bytes 393224 | tf_op jit(solution)/shard_map/ppermute | solution.py:174
  22.5 19.3 %collective-permute-start.7 = (bf16[512,128]{1,0:T(8,128)(2,1)S(1)}, bf16[512,128]{1,0:T(8,128)(2,1)S(1)}, u32[]{:S(2)}, u32[]{:S(2)}) collective-permute-start(bf16[512,128]{1,0:T(8,128)(2,1)S(1)} %bitcast.183), channel_id=1, source_target_pairs={{0,20},{4,24},{8,28},{12,0},{16,4},{20,8},{24,12},{28,16},{1,21},{... | collective-permute-start | bytes 393224 | tf_op jit(solution)/shard_map/ppermute | solution.py:174
  24.3 19.1 %collective-permute-start.8 = (bf16[512,128]{1,0:T(8,128)(2,1)S(1)}, bf16[512,128]{1,0:T(8,128)(2,1)S(1)}, u32[]{:S(2)}, u32[]{:S(2)}) collective-permute-start(bf16[512,128]{1,0:T(8,128)(2,1)S(1)} %bitcast.185), channel_id=1, source_target_pairs={{0,24},{4,28},{8,0},{12,4},{16,8},{20,12},{24,16},{28,20},{1,25},{... | collective-permute-start | bytes 393224 | tf_op jit(solution)/shard_map/ppermute | solution.py:174
  25.6 17.9 %collective-permute-start.9 = (bf16[512,128]{1,0:T(8,128)(2,1)S(1)}, bf16[512,128]{1,0:T(8,128)(2,1)S(1)}, u32[]{:S(2)}, u32[]{:S(2)}) collective-permute-start(bf16[512,128]{1,0:T(8,128)(2,1)S(1)} %bitcast.184), channel_id=1, source_target_pairs={{0,28},{4,0},{8,4},{12,8},{16,12},{20,16},{24,20},{28,24},{1,29},{... | collective-permute-start | bytes 393224 | tf_op jit(solution)/shard_map/ppermute | solution.py:174
  46.0 2.6 %copy-start.1 = (f32[512,512]{1,0:T(8,128)S(1)}, f32[512,512]{1,0:T(8,128)}, u32[]{:S(2)}) copy-start(f32[512,512]{1,0:T(8,128)} %get-tuple-element.70) | copy-start | bytes 3145732
  46.0 2.6 %copy-start.2 = (f32[512,512]{1,0:T(8,128)S(1)}, f32[512,512]{1,0:T(8,128)}, u32[]{:S(2)}) copy-start(f32[512,512]{1,0:T(8,128)} %get-tuple-element.71) | copy-start | bytes 3145732
  50.7 5.1 %collective-permute-start.10 = (bf16[64,1024]{1,0:T(8,128)(2,1)S(1)}, bf16[64,1024]{1,0:T(8,128)(2,1)S(1)}, u32[]{:S(2)}, u32[]{:S(2)}) collective-permute-start(bf16[64,1024]{1,0:T(8,128)(2,1)S(1)} %get-tuple-element.37), channel_id=1, source_target_pairs={{0,4},{4,8},{8,12},{12,16},{16,20},{20,24},{24,28},{28,0},{1,5},{5... | collective-permute-start | bytes 393224 | tf_op jit(solution)/shard_map/ppermute | solution.py:174
  50.8 7.1 %collective-permute-start.11 = (bf16[64,1024]{1,0:T(8,128)(2,1)S(1)}, bf16[64,1024]{1,0:T(8,128)(2,1)S(1)}, u32[]{:S(2)}, u32[]{:S(2)}) collective-permute-start(bf16[64,1024]{1,0:T(8,128)(2,1)S(1)} %get-tuple-element.36), channel_id=1, source_target_pairs={{0,8},{4,12},{8,16},{12,20},{16,24},{20,28},{24,0},{28,4},{1,9},{5... | collective-permute-start | bytes 393224 | tf_op jit(solution)/shard_map/ppermute | solution.py:174
  51.4 18.7 %collective-permute-start.12 = (bf16[64,1024]{1,0:T(8,128)(2,1)S(1)}, bf16[64,1024]{1,0:T(8,128)(2,1)S(1)}, u32[]{:S(2)}, u32[]{:S(2)}) collective-permute-start(bf16[64,1024]{1,0:T(8,128)(2,1)S(1)} %get-tuple-element.35), channel_id=1, source_target_pairs={{0,12},{4,16},{8,20},{12,24},{16,28},{20,0},{24,4},{28,8},{1,13},{... | collective-permute-start | bytes 393224 | tf_op jit(solution)/shard_map/ppermute | solution.py:174
  53.2 19.8 %collective-permute-start.13 = (bf16[64,1024]{1,0:T(8,128)(2,1)S(1)}, bf16[64,1024]{1,0:T(8,128)(2,1)S(1)}, u32[]{:S(2)}, u32[]{:S(2)}) collective-permute-start(bf16[64,1024]{1,0:T(8,128)(2,1)S(1)} %get-tuple-element.34), channel_id=1, source_target_pairs={{0,16},{4,20},{8,24},{12,28},{16,0},{20,4},{24,8},{28,12},{1,17},{... | collective-permute-start | bytes 393224 | tf_op jit(solution)/shard_map/ppermute | solution.py:174
  53.7 19.9 %collective-permute-start.14 = (bf16[64,1024]{1,0:T(8,128)(2,1)S(1)}, bf16[64,1024]{1,0:T(8,128)(2,1)S(1)}, u32[]{:S(2)}, u32[]{:S(2)}) collective-permute-start(bf16[64,1024]{1,0:T(8,128)(2,1)S(1)} %get-tuple-element.33), channel_id=1, source_target_pairs={{0,20},{4,24},{8,28},{12,0},{16,4},{20,8},{24,12},{28,16},{1,21},{... | collective-permute-start | bytes 393224 | tf_op jit(solution)/shard_map/ppermute | solution.py:174
  55.8 20.1 %collective-permute-start.15 = (bf16[64,1024]{1,0:T(8,128)(2,1)S(1)}, bf16[64,1024]{1,0:T(8,128)(2,1)S(1)}, u32[]{:S(2)}, u32[]{:S(2)}) collective-permute-start(bf16[64,1024]{1,0:T(8,128)(2,1)S(1)} %get-tuple-element.32), channel_id=1, source_target_pairs={{0,24},{4,28},{8,0},{12,4},{16,8},{20,12},{24,16},{28,20},{1,25},{... | collective-permute-start | bytes 393224 | tf_op jit(solution)/shard_map/ppermute | solution.py:174
  57.9 18.7 %collective-permute-start.16 = (bf16[64,1024]{1,0:T(8,128)(2,1)S(1)}, bf16[64,1024]{1,0:T(8,128)(2,1)S(1)}, u32[]{:S(2)}, u32[]{:S(2)}) collective-permute-start(bf16[64,1024]{1,0:T(8,128)(2,1)S(1)} %get-tuple-element.31), channel_id=1, source_target_pairs={{0,28},{4,0},{8,4},{12,8},{16,12},{20,16},{24,20},{28,24},{1,29},{... | collective-permute-start | bytes 393224 | tf_op jit(solution)/shard_map/ppermute | solution.py:174
  77.3 24.7 %collective-permute-start.18 = (bf16[8,64,1024]{2,1,0:T(8,128)(2,1)}, bf16[8,64,1024]{2,1,0:T(8,128)(2,1)S(1)}, u32[]{:S(2)}, u32[]{:S(2)}) collective-permute-start(bf16[8,64,1024]{2,1,0:T(8,128)(2,1)} %bitcast_dynamic-update-slice_fusion.8), channel_id=1, source_target_pairs={{0,2},{1,3},{2,0},{3,1},{4,6},{5,7},{6,4},{7,5},{8,10},{9,11},{10,... | collective-permute-start | bytes 3145736 | tf_op jit(solution)/shard_map/ppermute | solution.py:171
  78.5 25.4 %collective-permute-start.17 = (bf16[8,64,1024]{2,1,0:T(8,128)(2,1)}, bf16[8,64,1024]{2,1,0:T(8,128)(2,1)S(1)}, u32[]{:S(2)}, u32[]{:S(2)}) collective-permute-start(bf16[8,64,1024]{2,1,0:T(8,128)(2,1)} %bitcast_dynamic-update-slice_fusion.8), channel_id=1, source_target_pairs={{0,1},{1,0},{2,3},{3,2},{4,5},{5,4},{6,7},{7,6},{8,9},{9,8},{10,11... | collective-permute-start | bytes 3145736 | tf_op jit(solution)/shard_map/ppermute | solution.py:171
  102.0 20.6 %collective-permute-start.19 = (bf16[4,64,1024]{2,1,0:T(8,128)(2,1)S(1)}, bf16[4,64,1024]{2,1,0:T(8,128)(2,1)}, u32[]{:S(2)}, u32[]{:S(2)}) collective-permute-start(bf16[4,64,1024]{2,1,0:T(8,128)(2,1)S(1)} %slice.8), channel_id=1, source_target_pairs={{0,1},{1,0},{2,3},{3,2},{4,5},{5,4},{6,7},{7,6},{8,9},{9,8},{10,11... | collective-permute-start | bytes 1572872 | tf_op jit(solution)/shard_map/ppermute | solution.py:171
  104.0 18.7 %collective-permute-start.20 = (bf16[4,64,1024]{2,1,0:T(8,128)(2,1)S(1)}, bf16[4,64,1024]{2,1,0:T(8,128)(2,1)}, u32[]{:S(2)}, u32[]{:S(2)}) collective-permute-start(bf16[4,64,1024]{2,1,0:T(8,128)(2,1)S(1)} %slice.9), channel_id=1, source_target_pairs={{0,2},{1,3},{2,0},{3,1},{4,6},{5,7},{6,4},{7,5},{8,10},{9,11},{10,... | collective-permute-start | bytes 1572872 | tf_op jit(solution)/shard_map/ppermute | solution.py:171
  122.6 3.0 %copy-start.3 = (f32[512,1024]{1,0:T(8,128)S(1)}, f32[512,1024]{1,0:T(8,128)}, u32[]{:S(2)}) copy-start(f32[512,1024]{1,0:T(8,128)} %fusion.20) | copy-start | bytes 6291460
